TPU v7x, 32 devices: a whole 2x2x4 slice. The times are simulated.
32 devices in a mesh: ep: 4 (over y, x), tp: 8 (over z, core).
Axes of the slice: x: 2, y: 2, z: 4, core: 2. Of those that a mesh axis runs over, the one named last changes fastest.
Arguments:
- queries: bfloat16 [2048, 16, 128], P('ep', 'tp'), may hold values from -125 to 125
- keys: bfloat16 [2048, 16, 128], P('ep', 'tp'), may hold values from -9 to 9
- values: bfloat16 [2048, 16, 128], P('ep', 'tp'), may hold values from -6 to 6
- mixing: float32 [16], P('tp'), may hold values from 0.3 to 0.8
- head_gain: float32 [128], replicated, may hold values from 0.1 to 1.9
- out_weight: bfloat16 [16, 128, 2048], P('tp'), may hold values from -0.125 to 0.125
- tokens_b: bfloat16 [4096, 2048], P(('ep', 'tp')), may hold values from -6 to 6
- norm_gain: float32 [2048], replicated, may hold values from 0.1 to 1.9
- expert_ids: int32 [4096, 2], P(('ep', 'tp')), may hold values from 0 to 3, all different within a row; in each aligned block of 128 rows (0 to 127, 128 to 255, ...) at most 96 rows name the same one
- group_gate: float32 [4096], P(('ep', 'tp')), may hold values from 0.2 to 1
- expert_gate: float32 [4096, 2], P(('ep', 'tp')), may hold values from 0.1 to 0.9
- gate_weight: bfloat16 [4, 2048, 1024], P('ep', None, 'tp'), may hold values from -0.125 to 0.125
- up_weight: bfloat16 [4, 2048, 1024], P('ep', None, 'tp'), may hold values from -0.125 to 0.125
- down_weight: bfloat16 [4, 2048, 1024], P('ep', None, 'tp'), may hold values from -0.1875 to 0.1875
Outputs:
- mixed: bfloat16 [2048, 2048], P(('ep', 'tp'))
- routed: bfloat16 [4096, 2048], P(('ep', 'tp'))
Inputs may be any that keep to these rules, and one draw needn't show every extreme that they name: `expert_ids`: within each aligned block of 128 rows, no expert is named by more than 96 rows, and some block has an expert named by exactly 96 rows.
All inputs are finite; a program needn't handle non-finite values.
Results may differ from a plain program's by a relative error of at most 0.019.
Values may be sent and summed in bfloat16 or wider, within the bound.
A program may use at most 192 MiB of HBM per device.

v0:
```python
import math
import jax
import jax.numpy as jnp
from jax import lax
from jax.sharding import PartitionSpec as P

HEAD = 64


def attend_heads(queries, keys, values, mixing, head_gain):
    shard_rows = queries.shape[0]
    head_count = queries.shape[1]
    value_width = values.shape[2]
    query_start = lax.axis_index("ep") * shard_rows
    score_scale = 1.0 / math.sqrt(HEAD)
    query_pos = query_start + lax.iota(jnp.int32, shard_rows)

    def update(running, key_block, value_block, block_start):
        key_pos = block_start + lax.iota(jnp.int32, shard_rows)
        allowed = key_pos[None, :] <= query_pos[:, None]
        fresh = []
        for map_index in range(2):
            maximum, row_sum, numerator = running[3 * map_index : 3 * map_index + 3]
            offset = map_index * HEAD
            scores = (
                jnp.einsum(
                    "qhd,khd->hqk",
                    queries[:, :, offset : offset + HEAD],
                    key_block[:, :, offset : offset + HEAD],
                    preferred_element_type=jnp.float32,
                )
                * score_scale
            )
            scores = jnp.where(allowed[None], scores, -1e30)
            newmax = jnp.maximum(maximum, jnp.max(scores, axis=2))
            shrink = jnp.exp(maximum - newmax)
            weights = jnp.exp(scores - newmax[:, :, None])
            row_sum = row_sum * shrink + jnp.sum(weights, axis=2)
            numerator = numerator * shrink[:, :, None] + jnp.einsum(
                "hqk,khe->hqe",
                weights.astype(jnp.bfloat16),
                value_block,
                preferred_element_type=jnp.float32,
            )
            fresh += [newmax, row_sum, numerator]
        return tuple(fresh)

    floor_max = jnp.full((head_count, shard_rows), -1e30, jnp.float32)
    zero_sum = jnp.zeros((head_count, shard_rows), jnp.float32)
    zero_acc = jnp.zeros((head_count, shard_rows, value_width), jnp.float32)
    start_state = (floor_max, zero_sum, zero_acc, floor_max, zero_sum, zero_acc)
    running = start_state
    key_piece = lax.all_gather(keys, "ep", axis=0, tiled=True)
    value_piece = lax.all_gather(values, "ep", axis=0, tiled=True)
    blocks = key_piece.shape[0] // shard_rows
    key_blocks = key_piece.reshape(blocks, shard_rows, head_count, key_piece.shape[2])
    value_blocks = value_piece.reshape(blocks, shard_rows, head_count, value_width)

    def visit_block(state, inputs):
        key_block, value_block, block_index = inputs
        block_start = block_index * shard_rows
        state = lax.cond(
            block_start <= query_start + shard_rows - 1,
            lambda state_in: update(state_in, key_block, value_block, block_start),
            lambda state_in: state_in,
            state,
        )
        return (state, None)

    running, unused = lax.scan(
        visit_block, running, (key_blocks, value_blocks, lax.iota(jnp.int32, blocks))
    )
    state = running
    diff = state[2] / state[1][:, :, None] - mixing[:, None, None] * state[5] / state[4][:, :, None]
    normed = diff * lax.rsqrt(jnp.mean(diff * diff, axis=2, keepdims=True) + 1e-05) * head_gain
    return normed.astype(jnp.bfloat16)


def mixer_half(queries, keys, values, mixing, head_gain, out_weight):
    attended = attend_heads(queries, keys, values, mixing, head_gain)
    return lax.psum_scatter(
        jnp.einsum("hqe,hed->qd", attended, out_weight, preferred_element_type=jnp.float32).astype(
            jnp.bfloat16
        ),
        "tp",
        scatter_dimension=0,
        tiled=True,
    )


def expert_half(
    tokens_b, norm_gain, expert_ids, group_gate, expert_gate, gate_weight, up_weight, down_weight
):
    local_rows = tokens_b.shape[0]
    width = tokens_b.shape[1]
    top_count = expert_ids.shape[1]
    ep_count = lax.axis_size("ep")
    local_count = gate_weight.shape[0]
    expert_total = ep_count * local_count
    capacity = 3 * local_rows * top_count // (2 * expert_total)
    tokens_f = tokens_b.astype(jnp.float32)
    normed = (
        tokens_f
        * lax.rsqrt(jnp.mean(tokens_f * tokens_f, axis=1, keepdims=True) + 1e-06)
        * norm_gain
    ).astype(jnp.bfloat16)
    flat_ids = expert_ids.reshape(-1)
    one_hot = (flat_ids[:, None] == lax.iota(jnp.int32, expert_total)[None, :]).astype(jnp.int32)
    slot_rank = jnp.sum((jnp.cumsum(one_hot, axis=0) - one_hot) * one_hot, axis=1)
    slot_index = flat_ids * capacity + slot_rank
    owners = jnp.full((expert_total * capacity,), local_rows, jnp.int32)
    owners = owners.at[slot_index].set(lax.iota(jnp.int32, local_rows * top_count) // top_count)
    padded = jnp.concatenate([normed, jnp.zeros((1, width), jnp.bfloat16)], axis=0)
    outgoing = padded[owners].reshape(ep_count, local_count * capacity, width)
    incoming = lax.all_to_all(outgoing, "ep", split_axis=0, concat_axis=0, tiled=True)
    expert_rows = jnp.transpose(
        incoming.reshape(ep_count, local_count, capacity, width), (1, 0, 2, 3)
    )
    expert_rows = expert_rows.reshape(local_count, ep_count * capacity, width)
    piece_gate = lax.all_gather(gate_weight, "tp", axis=2, tiled=True)
    piece_up = lax.all_gather(up_weight, "tp", axis=2, tiled=True)
    piece_down = lax.all_gather(down_weight, "tp", axis=2, tiled=True)
    gate_part = jnp.einsum(
        "jrd,jdf->jrf", expert_rows, piece_gate, preferred_element_type=jnp.float32
    )
    up_part = jnp.einsum("jrd,jdf->jrf", expert_rows, piece_up, preferred_element_type=jnp.float32)
    hidden = (jax.nn.silu(gate_part) * up_part).astype(jnp.bfloat16)
    expert_out = jnp.einsum(
        "jrf,jdf->jrd", hidden, piece_down, preferred_element_type=jnp.float32
    ).astype(jnp.bfloat16)
    outbound = jnp.transpose(
        expert_out.reshape(local_count, ep_count, capacity, width), (1, 0, 2, 3)
    )
    outbound = outbound.reshape(ep_count, local_count * capacity, width)
    returned = lax.all_to_all(outbound, "ep", split_axis=0, concat_axis=0, tiled=True).reshape(
        expert_total * capacity, width
    )
    picked = returned[slot_index].reshape(local_rows, top_count, width).astype(jnp.float32)
    route_weight = group_gate[:, None] * expert_gate
    return jnp.sum(route_weight[:, :, None] * picked, axis=1).astype(jnp.bfloat16)


def per_device(
    queries,
    keys,
    values,
    mixing,
    head_gain,
    out_weight,
    tokens_b,
    norm_gain,
    expert_ids,
    group_gate,
    expert_gate,
    gate_weight,
    up_weight,
    down_weight,
):
    mixed = mixer_half(queries, keys, values, mixing, head_gain, out_weight)
    routed = expert_half(
        tokens_b,
        norm_gain,
        expert_ids,
        group_gate,
        expert_gate,
        gate_weight,
        up_weight,
        down_weight,
    )
    return (mixed, routed)


def solution(mesh):
    placed = (
        P("ep", "tp", None),
        P("ep", "tp", None),
        P("ep", "tp", None),
        P("tp"),
        P(),
        P("tp", None, None),
        P(("ep", "tp"), None),
        P(),
        P(("ep", "tp"), None),
        P(("ep", "tp")),
        P(("ep", "tp"), None),
        P("ep", None, "tp"),
        P("ep", None, "tp"),
        P("ep", None, "tp"),
    )
    return jax.shard_map(
        per_device,
        mesh=mesh,
        in_specs=placed,
        out_specs=(P(("ep", "tp"), None), P(("ep", "tp"), None)),
        check_vma=False,
    )
```

profile of v0, /device:TPU:0, one launch (start us, length us, event | category | flops | bytes accessed | tf_op | source)
XLA Modules:
  0.0 260.2 jit_solution(6079203360803837472)
XLA Ops:
  7.2 0.0 copy-start
  7.2 0.0 all-gather.6.cloned.1.call-start
  7.3 1.8 copy.24
  9.1 0.0 all-gather.6.cloned.1.call-update
  9.1 0.0 all-gather.8.cloned.1.call-start
  9.1 1.7 copy.25
  10.8 0.0 all-gather.8.cloned.1.call-update
  10.8 0.0 all-gather.10.cloned.1.call-start
  10.9 0.7 all-gather.10.cloned.1.call-update
  11.6 0.0 all-gather.12.cloned.1.call-start
  11.6 0.5 all-gather.12.cloned.1.call-update
  12.2 0.0 all-gather.14.cloned.1.call-start
  12.2 0.5 all-gather.14.cloned.1.call-update
  12.7 0.0 reduce-scatter.2.cloned.1.call-start
  12.8 0.1 copy.31
  12.9 0.1 eq.29
  13.1 0.1 eq.25
  13.2 0.2 copy.27
  13.4 1.2 reduce-window.6
  14.6 0.1 slice.34
  14.7 0.1 copy.33
  14.9 0.1 copy.34
  15.0 0.1 copy.30
  15.1 0.1 mul.169
  15.2 0.1 add_bitcast_fusion
  15.3 1.4 scatter_custom_fusion
  16.7 0.2 fusion.31
  17.0 1.0 fusion.33
  17.9 21.8 %all-gather.6.cloned.1.call-done = bf16[2048,2,128]{2,0,1:T(8,128)(2,1)} async-done(((bf16[512,2,128]{2,0,1:T(8,128)(2,1)}), bf16[2048,2,128]{2,0,1:T(8,128)(2,1)}) %all-gather.6.cloned.1.call-update) | async-done | bytes 1048592 | tf_op jit(solution)/shard_map/all_gather | solution.py:53
  39.7 2.3 copy.26
  42.0 26.1 %all-gather.8.cloned.1.call-done = bf16[2048,2,128]{2,0,1:T(8,128)(2,1)} async-done(((bf16[512,2,128]{2,0,1:T(8,128)(2,1)}), bf16[2048,2,128]{2,0,1:T(8,128)(2,1)}) %all-gather.8.cloned.1.call-update) | async-done | bytes 1048592 | tf_op jit(solution)/shard_map/all_gather | solution.py:54
  68.1 1.3 copy.28
  69.5 0.0 copy-start.8
  69.5 0.0 copy-start.9
  69.5 9.8 %while.23 = (s32[]{:T(128)}, f32[2,512]{1,0:T(2,128)S(1)}, f32[2,512]{1,0:T(2,128)S(1)}, f32[2,512,128]{2,1,0:T(8,128)S(1)}, f32[2,512]{1,0:T(2,128)S(1)}, /*ind...) while((s32[]{:T(128)}, f32[2,512]{1,0:T(2,128)S(1)}, ...), condition=%wide.region_7.8_spmd.clone, body=%wide.region_0.7_spmd.clone.sunk | while | flops 410784768 | bytes 17183128 | solution.py:70
  69.6 0.6 dynamic_slice.36
  70.8 4.6 %conditional.3 = ((f32[2,512]{1,0:T(2,128)S(1)}, f32[2,512]{1,0:T(2,128)S(1)}, f32[2,512,128]{2,1,0:T(8,128)S(1)}, f32[2,512]{1,0:T(2,128)S(1)}, f32[2,512]{1,0:T(2,128)S(1)}, /*index=5*/f32[2,512,128]{2,1,0:T(8,128)S(1)})) conditional(s32[]{:T(128)} %convert_element_type.87, (f32[2,512]{1,0:T(2,128)S(1)}, f32[2,512]{1,0:T(2,128)S(1)}, ...), branch_computations={%region_1.1_spmd, %region_2.6_spmd} | conditional | flops 410784768 | bytes 17180748 | solution.py:62
  70.8 1.0 dynamic-slice_bitcast_fusion
  71.8 0.2 broadcast_compare_fusion
  72.1 0.6 fusion.45
  72.7 0.3 fusion.3
  73.0 0.6 fusion.46
  73.6 0.3 fusion.5
  74.0 0.7 convolution_add_fusion
  74.7 0.7 convolution_add_fusion.1
  75.5 0.6 dynamic_slice.36
  76.8 0.6 dynamic_slice.36
  78.1 0.6 dynamic_slice.36
  79.4 0.5 multiply_reduce_fusion.1
  79.9 0.0 copy-start.2
  79.9 2.1 bitcast_convert_fusion
  82.0 0.0 reduce-scatter.2.cloned.1.call-update
  82.2 2.5 gather_fusion
  84.6 36.1 %all_to_all.10 = bf16[4,96,2048]{2,1,0:T(8,128)(2,1)} all-to-all(bf16[4,96,2048]{2,1,0:T(8,128)(2,1)S(1)} %bitcast.62), channel_id=1, replica_groups=mesh['ep'=4,'tp'=8] {'ep'}, dimensions={0} | all-to-all | bytes 3145728 | tf_op jit(solution)/shard_map/all_to_all | solution.py:115
  120.7 5.7 %fusion.24 = f32[384,1024]{1,0:T(8,128)} fusion(bf16[384,2048]{1,0:T(8,128)(2,1)} %bitcast.63, bf16[1,2048,1024]{2,1,0:T(8,128)(2,1)} %all-gather.10.cloned.1.call-done), kind=kOutput, calls=%fused_computation.38 | convolution fusion | flops 1610612736 | bytes 7340032 | tf_op jit(solution)/shard_map/jrd,jdf->jrf/dot_general | solution.py:123
  126.4 38.6 %all-gather.12.cloned.1.call-done = bf16[1,2048,1024]{2,1,0:T(8,128)(2,1)} async-done(((bf16[1,2048,128]{2,1,0:T(8,128)(2,1)}), bf16[1,2048,1024]{2,1,0:T(8,128)(2,1)}) %all-gather.12.cloned.1.call-update) | async-done | bytes 4194320 | tf_op jit(solution)/shard_map/all_gather | solution.py:121
  165.0 47.5 %all-gather.14.cloned.1.call-done = bf16[1,2048,1024]{2,1,0:T(8,128)(2,1)} async-done(((bf16[1,2048,128]{2,1,0:T(8,128)(2,1)}), bf16[1,2048,1024]{2,1,0:T(8,128)(2,1)}) %all-gather.14.cloned.1.call-update) | async-done | bytes 4194320 | tf_op jit(solution)/shard_map/all_gather | solution.py:122
  212.5 8.6 %fusion.26 = bf16[384,2048]{1,0:T(8,128)(2,1)} fusion(bf16[1,2048,1024]{2,1,0:T(8,128)(2,1)} %all-gather.14.cloned.1.call-done, f32[384,1024]{1,0:T(8,128)} %fusion.24, bf16[384,2048]{1,0:T(8,128)(2,1)S(1)} %bitcast.64, bf16[1,2048,1024]{2,1,0:T(8,128)(2,1)} %all-gather.12.cloned.1.call-done), kind=kOutput, calls=%fused_computation.41 | convolution fusion | flops 3224371200 | bytes 13107200 | tf_op jit(solution)/shard_map/jrf,jdf->jrd/dot_general | solution.py:128
  221.1 3.8 %all-to-all-start.1 = ((bf16[4,96,2048]{2,1,0:T(8,128)(2,1)}), bf16[4,96,2048]{2,1,0:T(8,128)(2,1)S(1)}, u32[]{:S(2)}, u32[]{:S(2)}) async-start(bf16[4,96,2048]{2,1,0:T(8,128)(2,1)} %bitcast.65), calls=%async_computation.2 | async-start | bytes 3145728 | tf_op jit(solution)/shard_map/all_to_all | solution.py:135
  224.9 0.1 copy.29
  225.0 19.7 %all-to-all-done.1 = bf16[4,96,2048]{2,1,0:T(8,128)(2,1)S(1)} async-done(((bf16[4,96,2048]{2,1,0:T(8,128)(2,1)}), bf16[4,96,2048]{2,1,0:T(8,128)(2,1)S(1)}, u32[]{:S(2)}, u32[]{:S(2)}) %all-to-all-start.1) | async-done | bytes 1572896 | tf_op jit(solution)/shard_map/all_to_all | solution.py:135
  244.7 2.3 gather_fusion.1
  247.1 2.4 reshape.163
  249.4 3.9 %multiply_reduce_fusion = bf16[128,2048]{1,0:T(8,128)(2,1)} fusion(f32[128,2,2048]{2,1,0:T(2,128)S(1)} %reshape.163, f32[128,2]{1,0:T(8,128)S(1)} %copy.29), kind=kLoop, calls=%fused_computation.42 | loop fusion | flops 786432 | bytes 2622464 | tf_op jit(solution)/shard_map/reduce_sum | solution.py:140
  (55 shorter events, 0.4 us)
Async XLA Ops:
  7.2 72.7 %copy-start = (bf16[2,128,2048]{2,1,0:T(8,128)(2,1)S(1)}, bf16[2,128,2048]{2,1,0:T(8,128)(2,1)}, u32[]{:S(2)}) copy-start(bf16[2,128,2048]{2,1,0:T(8,128)(2,1)} %param.23) | copy-start | bytes 3145732
  7.2 5.6 %copy-start.6 = (s32[128,2]{0,1:T(2,128)S(1)}, s32[128,2]{0,1:T(2,128)}, u32[]{:S(2)}) copy-start(s32[128,2]{0,1:T(2,128)} %param.26) | copy-start | bytes 3076
  7.2 6.0 %copy-start.4 = (bf16[512,2,128]{2,1,0:T(2,128)(2,1)S(1)}, bf16[512,2,128]{2,1,0:T(2,128)(2,1)}, u32[]{:S(2)}) copy-start(bf16[512,2,128]{2,1,0:T(2,128)(2,1)} %param.18) | copy-start | bytes 786436
  7.2 9.5 %copy-start.1 = (bf16[128,2048]{1,0:T(8,128)(2,1)S(1)}, bf16[128,2048]{1,0:T(8,128)(2,1)}, u32[]{:S(2)}) copy-start(bf16[128,2048]{1,0:T(8,128)(2,1)} %param.24) | copy-start | bytes 1572868
  7.2 32.5 %all-gather.6.cloned.1.call-start = ((), (), s32[]{:S(2)}) async-start(), calls=%async_computation.3 | async-start | bytes 1310720 | tf_op jit(solution)/shard_map/all_gather | solution.py:53
  9.1 7.9 %copy-start.5 = (f32[2048]{0:T(1024)S(1)}, f32[2048]{0:T(1024)}, u32[]{:S(2)}) copy-start(f32[2048]{0:T(1024)} %param.25) | copy-start | bytes 24580
  9.1 59.0 %all-gather.8.cloned.1.call-start = ((), (), s32[]{:S(2)}) async-start(), calls=%async_computation.4 | async-start | bytes 1310720 | tf_op jit(solution)/shard_map/all_gather | solution.py:54
  10.8 109.8 %all-gather.10.cloned.1.call-start = ((), (), s32[]{:S(2)}) async-start(), calls=%async_computation.6 | async-start | bytes 4718592 | tf_op jit(solution)/shard_map/all_gather | solution.py:120
  11.6 153.4 %all-gather.12.cloned.1.call-start = ((), (), s32[]{:S(2)}) async-start(), calls=%async_computation.7 | async-start | bytes 4718592 | tf_op jit(solution)/shard_map/all_gather | solution.py:121
  12.2 200.3 %all-gather.14.cloned.1.call-start = ((), (), s32[]{:S(2)}) async-start(), calls=%async_computation.8 | async-start | bytes 4718592 | tf_op jit(solution)/shard_map/all_gather | solution.py:122
  12.7 240.6 %reduce-scatter.2.cloned.1.call-start = ((), (), s32[]{:S(2)}) async-start(), calls=%async_computation.5 | async-start | bytes 2359296 | tf_op jit(solution)/shard_map/reduce_scatter | solution.py:81
  69.5 9.9 %copy-start.8 = (f32[2]{0:T(128)S(1)}, f32[2]{0:T(128)}, u32[]{:S(2)}) copy-start(f32[2]{0:T(128)} %param.21) | copy-start | bytes 28
  69.5 10.4 %copy-start.9 = (f32[128]{0:T(128)S(1)}, f32[128]{0:T(128)}, u32[]{:S(2)}) copy-start(f32[128]{0:T(128)} %param.22) | copy-start | bytes 1540
  79.9 2.2 copy-start.2
  120.7 91.8 %copy-start.3 = (bf16[4,96,2048]{2,1,0:T(8,128)(2,1)S(1)}, bf16[4,96,2048]{2,1,0:T(8,128)(2,1)}, u32[]{:S(2)}) copy-start(bf16[4,96,2048]{2,1,0:T(8,128)(2,1)} %all_to_all.10) | copy-start | bytes 4718596
  221.1 3.8 %copy-start.7 = (f32[128,2]{0,1:T(2,128)S(1)}, f32[128,2]{0,1:T(2,128)}, u32[]{:S(2)}) copy-start(f32[128,2]{0,1:T(2,128)} %param.28) | copy-start | bytes 3076
  221.1 3.8 %copy-start.10 = (f32[128]{0:T(128)S(1)}, f32[128]{0:T(128)}, u32[]{:S(2)}) copy-start(f32[128]{0:T(128)} %param.27) | copy-start | bytes 1540
  221.1 23.6 %all-to-all-start.1 = ((bf16[4,96,2048]{2,1,0:T(8,128)(2,1)}), bf16[4,96,2048]{2,1,0:T(8,128)(2,1)S(1)}, u32[]{:S(2)}, u32[]{:S(2)}) async-start(bf16[4,96,2048]{2,1,0:T(8,128)(2,1)} %bitcast.65), calls=%async_computation.2 | async-start | bytes 3145728 | tf_op jit(solution)/shard_map/all_to_all | solution.py:135
Sparse Core Ops, SparseCore 0:
  10.4 29.2 all-gather.5
  41.5 26.4 all-gather.7
  69.7 47.8 all-gather.9
  119.0 45.9 all-gather.11
  166.4 45.9 all-gather.13
  215.2 34.1 reduce-scatter.1
where the time goes:
time: 261 us; the launch traced here: 260 us
  waiting for transfers between devices  155 us (59%)
  blocking collectives  36.1 us (14%)
  local copies, waits for them, and re-layouts  20.4 us (8%)
  matrix products  19.2 us (7%)
  between operations  14.4 us (6%)
  other arithmetic  7.89 us (3%)
  starting transfers between devices  4.02 us (2%)
  loops' own time  2.93 us (1%)
    all_gather x1, waiting for transfers between devices, expert_half(): piece_down = lax.all_gather(down_weight, 'tp', axis=2, tiled=True)  47.5 us
    all_gather x1, waiting for transfers between devices, expert_half(): piece_up = lax.all_gather(up_weight, 'tp', axis=2, tiled=True)  38.6 us
    all_to_all x1, blocking collectives, expert_half(): lax.all_to_all(outgoing, 'ep', split_axis=0, concat_axis=0, tiled=True)  36.1 us
    all_gather x1, waiting for transfers between devices, attend_heads(): value_piece = lax.all_gather(values, 'ep', axis=0, tiled=True)  26.1 us
    all_gather x1, waiting for transfers between devices, attend_heads(): key_piece = lax.all_gather(keys, 'ep', axis=0, tiled=True)  21.8 us
    all_to_all x1, waiting for transfers between devices, expert_half(): lax.all_to_all(outbound, 'ep', split_axis=0, concat_axis=0, tiled=True)  19.7 us
    dot_general x1, matrix products, expert_half(): jnp.einsum('jrf,jdf->jrd', hidden, piece_down, preferred_element_type=jnp...  8.63 us
    unnamed x28, local copies, waits for them, and re-layouts  7.42 us
  transfers between devices with their start and end apart: 7, of which 5 were waited for; matrix products, arithmetic and copies ran while one was open for 18% of the time, Pallas kernels for 0%

commit v1 on v0

--- a/solution.py
+++ b/solution.py
@@ -5,6 +5,22 @@
 from jax.sharding import PartitionSpec as P
 
 HEAD = 64
+
+
+def _change_body(field, link_axis, xin):
+    f_next, reached, res = (lax.axis_size(link_axis), lax.axis_index(link_axis), field.shape[2])
+    buffer = [(src_i, (src_i + 1) % f_next) for src_i in range(f_next)]
+    inter = f_next // 2
+    kept_rows = [(src_i, (src_i - 1) % f_next) for src_i in range(f_next)]
+    long_array = small = field
+    a_now = xin(field, reached * res)
+    for k in range(1, inter + 1):
+        long_array = lax.ppermute(long_array, link_axis, buffer)
+        if k < f_next - inter:
+            small = lax.ppermute(small, link_axis, kept_rows)
+            a_now = a_now + xin(small, (reached + k) % f_next * res)
+        a_now = a_now + xin(long_array, (reached - k) % f_next * res)
+    return a_now
 
 
 def attend_heads(queries, keys, values, mixing, head_gain):
@@ -119,14 +135,20 @@
     expert_rows = expert_rows.reshape(local_count, ep_count * capacity, width)
     piece_gate = lax.all_gather(gate_weight, "tp", axis=2, tiled=True)
     piece_up = lax.all_gather(up_weight, "tp", axis=2, tiled=True)
-    piece_down = lax.all_gather(down_weight, "tp", axis=2, tiled=True)
     gate_part = jnp.einsum(
         "jrd,jdf->jrf", expert_rows, piece_gate, preferred_element_type=jnp.float32
     )
     up_part = jnp.einsum("jrd,jdf->jrf", expert_rows, piece_up, preferred_element_type=jnp.float32)
     hidden = (jax.nn.silu(gate_part) * up_part).astype(jnp.bfloat16)
-    expert_out = jnp.einsum(
-        "jrf,jdf->jrd", hidden, piece_down, preferred_element_type=jnp.float32
+    expert_out = _change_body(
+        down_weight,
+        "tp",
+        lambda own_block, at: jnp.einsum(
+            "jrf,jdf->jrd",
+            lax.dynamic_slice_in_dim(hidden, at, own_block.shape[2], axis=2),
+            own_block,
+            preferred_element_type=jnp.float32,
+        ),
     ).astype(jnp.bfloat16)
     outbound = jnp.transpose(
         expert_out.reshape(local_count, ep_count, capacity, width), (1, 0, 2, 3)

time: 261 us -> 231 us (0.89)
  blocking collectives: 36.1 us -> 0 us
  starting transfers between devices: 4.02 us -> 21.5 us
  waiting for transfers between devices: 155 us -> 138 us
  matrix products: 19.2 us -> 25.7 us
    all_gather x1 -> x0, waiting for transfers between devices: 47.5 us -> none  [expert_half(): piece_down = lax.all_gather(down_weight, 'tp', axis=2, tiled=True)]
    all_to_all x1 -> x0, blocking collectives: 36.1 us -> none  [expert_half(): lax.all_to_all(outgoing, 'ep', split_axis=0, concat_axis=0, tiled=True)]
    all_gather x1, waiting for transfers between devices: 0.01 us -> 35.2 us  [expert_half(): piece_gate = lax.all_gather(gate_weight, 'tp', axis=2, tiled=True)]
    all_gather x1, waiting for transfers between devices: 21.8 us -> 0.01 us  [attend_heads(): key_piece = lax.all_gather(keys, 'ep', axis=0, tiled=True)]
    ppermute x0 -> x7, waiting for transfers between devices: none -> 13.1 us  [the longest x4 13.1 us: _change_body(): long_array = lax.ppermute(long_array, link_axis, buffer)]
    ppermute x0 -> x7, starting transfers between devices: none -> 11.5 us  [the longest x3 11 us: _change_body(): small = lax.ppermute(small, link_axis, kept_rows)]
    dot_general x1 -> x9, matrix products: 8.63 us -> 16.4 us  [the longest x8 11.8 us: expert_half(): jnp.einsum('jrf,jdf->jrd', lax.dynamic_slice_in_dim(hidden, at, own_block...]
    all_to_all x0 -> x1, starting transfers between devices: none -> 5.85 us  [expert_half(): lax.all_to_all(outgoing, 'ep', split_axis=0, concat_axis=0, tiled=True)]
  transfers between devices with their start and end apart: 7 -> 14, of which waited for: 5 -> 6; matrix products, arithmetic and copies ran while one was open for 18% -> 23% of each run, Pallas kernels for 0% -> 0%
where the time goes in v1:
time: 231 us
  waiting for transfers between devices  138 us (60%)
  matrix products  25.7 us (11%)
  local copies, waits for them, and re-layouts  21.5 us (9%)
  starting transfers between devices  21.5 us (9%)
  between operations  14.3 us (6%)
  other arithmetic  7.09 us (3%)
  loops' own time  3.11 us (1%)
    all_gather x1, waiting for transfers between devices, expert_half(): piece_up = lax.all_gather(up_weight, 'tp', axis=2, tiled=True)  43 us
    all_gather x1, waiting for transfers between devices, expert_half(): piece_gate = lax.all_gather(gate_weight, 'tp', axis=2, tiled=True)  35.2 us
    all_gather x1, waiting for transfers between devices, attend_heads(): value_piece = lax.all_gather(values, 'ep', axis=0, tiled=True)  25.4 us
    all_to_all x1, waiting for transfers between devices, expert_half(): lax.all_to_all(outbound, 'ep', split_axis=0, concat_axis=0, tiled=True)  19.5 us
    ppermute x4, waiting for transfers between devices, _change_body(): long_array = lax.ppermute(long_array, link_axis, buffer)  13.1 us
    dot_general x8, matrix products, expert_half(): jnp.einsum('jrf,jdf->jrd', lax.dynamic_slice_in_dim(hidden, at, own_block...  11.8 us
    ppermute x3, starting transfers between devices, _change_body(): small = lax.ppermute(small, link_axis, kept_rows)  11 us
    unnamed x36, local copies, waits for them, and re-layouts  7.9 us
  transfers between devices with their start and end apart: 14, of which 6 were waited for; matrix products, arithmetic and copies ran while one was open for 23% of the time, Pallas kernels for 0%

profile of v1, /device:TPU:0, one launch (start us, length us, event | category | flops | bytes accessed | tf_op | source)
XLA Modules:
  0.0 230.7 jit_solution(10217454517277534988)
XLA Ops:
  7.3 1.8 copy.24
  9.2 1.7 copy.25
  10.9 0.7 all-gather.9.cloned.1.call-update
  11.7 0.5 all-gather.11.cloned.1.call-update
  12.2 0.5 collective-permute-start.1
  12.8 4.1 %collective-permute-start = (bf16[1,2048,128]{2,1,0:T(8,128)(2,1)S(1)}, bf16[1,2048,128]{2,1,0:T(8,128)(2,1)S(1)}, u32[]{:S(2)}, u32[]{:S(2)}) collective-permute-start(bf16[1,2048,128]{2,1,0:T(8,128)(2,1)S(1)} %copy-done.2), channel_id=1, source_target_pairs={{0,7},{1,0},{2,1},{3,2},{4,3},{5,4},{6,5},{7,6},{8,15},{9,8},{10,9... | collective-permute-start | bytes 1572872 | tf_op jit(solution)/shard_map/ppermute | solution.py:20
  16.9 0.1 copy.31
  17.0 0.1 eq.37
  17.1 0.1 eq.33
  17.3 1.2 reduce-window.6
  18.5 0.1 slice.34
  18.6 0.1 copy.33
  18.7 0.1 copy.34
  18.8 0.1 copy.30
  18.9 0.1 mul.193
  19.1 0.2 fusion.26
  19.3 0.1 add_bitcast_fusion
  19.4 7.3 %collective-permute-done.1 = bf16[1,2048,128]{2,1,0:T(8,128)(2,1)S(1)} collective-permute-done((bf16[1,2048,128]{2,1,0:T(8,128)(2,1)S(1)}, bf16[1,2048,128]{2,1,0:T(8,128)(2,1)S(1)}, u32[]{:S(2)}, u32[]{:S(2)}) %collective-permute-start.1) | collective-permute-done | bytes 524320 | tf_op jit(solution)/shard_map/ppermute | solution.py:18
  26.7 1.4 scatter_custom_fusion
  28.1 0.2 fusion.28
  28.3 3.6 %collective-permute-start.2 = (bf16[1,2048,128]{2,1,0:T(8,128)(2,1)S(1)}, bf16[1,2048,128]{2,1,0:T(8,128)(2,1)}, u32[]{:S(2)}, u32[]{:S(2)}) collective-permute-start(bf16[1,2048,128]{2,1,0:T(8,128)(2,1)S(1)} %collective-permute-done), channel_id=1, source_target_pairs={{0,7},{1,0},{2,1},{3,2},{4,3},{5,4},{6,5},{7,6},{8,15},{9,8},{10,9... | collective-permute-start | bytes 1572872 | tf_op jit(solution)/shard_map/ppermute | solution.py:20
  31.9 5.8 %collective-permute-done.3 = bf16[1,2048,128]{2,1,0:T(8,128)(2,1)} collective-permute-done((bf16[1,2048,128]{2,1,0:T(8,128)(2,1)S(1)}, bf16[1,2048,128]{2,1,0:T(8,128)(2,1)}, u32[]{:S(2)}, u32[]{:S(2)}) %collective-permute-start.3) | collective-permute-done | bytes 524320 | tf_op jit(solution)/shard_map/ppermute | solution.py:18
  37.8 3.1 %gather_fusion = bf16[384,2048]{1,0:T(8,128)(2,1)} fusion(bf16[129,2048]{1,0:T(8,128)(2,1)S(1)} %concatenate.3, s32[1024]{0:T(1024)S(1)} %pad_clamp_fusion.1), kind=kCustom, calls=%fused_computation | custom fusion | bytes 3147264 | tf_op jit(solution)/shard_map/gather | solution.py:130
  40.9 5.8 %all-to-all-start = ((bf16[4,96,2048]{2,1,0:T(8,128)(2,1)}), bf16[4,96,2048]{2,1,0:T(8,128)(2,1)}, u32[]{:S(2)}, u32[]{:S(2)}) async-start(bf16[4,96,2048]{2,1,0:T(8,128)(2,1)} %bitcast.11), calls=%async_computation.1 | async-start | bytes 3145728 | tf_op jit(solution)/shard_map/all_to_all | solution.py:131
  46.8 0.2 copy.27
  47.0 3.3 %collective-permute-start.4 = (bf16[1,2048,128]{2,1,0:T(8,128)(2,1)}, bf16[1,2048,128]{2,1,0:T(8,128)(2,1)}, u32[]{:S(2)}, u32[]{:S(2)}) collective-permute-start(bf16[1,2048,128]{2,1,0:T(8,128)(2,1)} %collective-permute-done.2), channel_id=1, source_target_pairs={{0,7},{1,0},{2,1},{3,2},{4,3},{5,4},{6,5},{7,6},{8,15},{9,8},{10,9... | collective-permute-start | bytes 1572872 | tf_op jit(solution)/shard_map/ppermute | solution.py:20
  50.3 2.3 copy.26
  52.6 25.4 %all-gather.7.cloned.1.call-done = bf16[2048,2,128]{2,0,1:T(8,128)(2,1)} async-done(((bf16[512,2,128]{2,0,1:T(8,128)(2,1)}), bf16[2048,2,128]{2,0,1:T(8,128)(2,1)}) %all-gather.7.cloned.1.call-update) | async-done | bytes 1048592 | tf_op jit(solution)/shard_map/all_gather | solution.py:70
  78.0 1.3 copy.28
  79.4 10.0 %while.23 = (s32[]{:T(128)}, f32[2,512]{1,0:T(2,128)S(1)}, f32[2,512]{1,0:T(2,128)S(1)}, f32[2,512,128]{2,1,0:T(8,128)S(1)}, f32[2,512]{1,0:T(2,128)S(1)}, /*ind...) while((s32[]{:T(128)}, f32[2,512]{1,0:T(2,128)S(1)}, ...), condition=%wide.region_7.8_spmd.clone, body=%wide.region_0.7_spmd.clone.sunk | while | flops 410784768 | bytes 17183128 | solution.py:86
  79.5 0.6 dynamic_slice.44
  80.7 4.6 %conditional.3 = ((f32[2,512]{1,0:T(2,128)S(1)}, f32[2,512]{1,0:T(2,128)S(1)}, f32[2,512,128]{2,1,0:T(8,128)S(1)}, f32[2,512]{1,0:T(2,128)S(1)}, f32[2,512]{1,0:T(2,128)S(1)}, /*index=5*/f32[2,512,128]{2,1,0:T(8,128)S(1)})) conditional(s32[]{:T(128)} %convert_element_type.85, (f32[2,512]{1,0:T(2,128)S(1)}, f32[2,512]{1,0:T(2,128)S(1)}, ...), branch_computations={%region_1.1_spmd, %region_2.6_spmd} | conditional | flops 410784768 | bytes 17180748 | solution.py:78
  80.7 1.0 dynamic-slice_bitcast_fusion
  81.7 0.2 broadcast_compare_fusion
  82.0 0.6 fusion.67
  82.6 0.3 fusion.3
  82.9 0.6 fusion.68
  83.5 0.3 fusion.5
  83.9 0.7 convolution_add_fusion
  84.6 0.7 convolution_add_fusion.1
  85.4 0.6 dynamic_slice.44
  86.7 0.6 dynamic_slice.44
  88.0 0.6 dynamic_slice.44
  89.5 0.5 multiply_reduce_fusion.1
  90.0 2.2 bitcast_convert_fusion
  92.2 35.2 %all-gather.9.cloned.1.call-done = bf16[1,2048,1024]{2,1,0:T(8,128)(2,1)} async-done(((bf16[1,2048,128]{2,1,0:T(8,128)(2,1)}), bf16[1,2048,1024]{2,1,0:T(8,128)(2,1)}) %all-gather.9.cloned.1.call-update) | async-done | bytes 4194320 | tf_op jit(solution)/shard_map/all_gather | solution.py:136
  127.4 4.4 %fusion.22 = f32[384,1024]{1,0:T(8,128)S(1)} fusion(bf16[384,2048]{1,0:T(8,128)(2,1)} %bitcast.12, bf16[1,2048,1024]{2,1,0:T(8,128)(2,1)} %all-gather.9.cloned.1.call-done), kind=kOutput, calls=%fused_computation.36 | convolution fusion | flops 1610612736 | bytes 7340032 | tf_op jit(solution)/shard_map/jrd,jdf->jrf/dot_general | solution.py:138
  131.9 43.0 %all-gather.11.cloned.1.call-done = bf16[1,2048,1024]{2,1,0:T(8,128)(2,1)} async-done(((bf16[1,2048,128]{2,1,0:T(8,128)(2,1)}), bf16[1,2048,1024]{2,1,0:T(8,128)(2,1)}) %all-gather.11.cloned.1.call-update) | async-done | bytes 4194320 | tf_op jit(solution)/shard_map/all_gather | solution.py:137
  174.9 4.6 %multiply_convert_fusion = bf16[384,1024]{1,0:T(8,128)(2,1)S(1)} fusion(f32[384,1024]{1,0:T(8,128)S(1)} %fusion.22, bf16[384,2048]{1,0:T(8,128)(2,1)} %bitcast.12, bf16[1,2048,1024]{2,1,0:T(8,128)(2,1)} %all-gather.11.cloned.1.call-done), kind=kOutput, calls=%fused_computation.41 | convolution fusion | flops 1612972032 | bytes 8126464 | tf_op jit(solution)/shard_map/jrd,jdf->jrf/dot_general | solution.py:141
  179.5 0.6 fusion.42
  180.1 1.6 fusion.30
  181.7 1.6 fusion.34
  183.4 1.7 fusion.36
  185.1 0.6 fusion.38
  185.6 0.5 copy-done.7
  186.1 0.6 fusion.40
  186.7 1.6 fusion.32
  188.3 3.5 %add_convert_fusion = bf16[384,2048]{1,0:T(8,128)(2,1)} fusion(f32[384,2048]{1,0:T(8,128)S(1)} %fusion.30, f32[384,2048]{1,0:T(8,128)S(1)} %fusion.32, f32[384,2048]{1,0:T(8,128)S(1)} %fusion.34, f32[384,2048]{1,0:T(8,128)S(1)} %fusion.36, f32[384,2048]{1,0:T(8,128)S(1)} %fusion.38, f32[384,2048]{1,0:T(8,128)S(1)} %fusion.42, f32[384,2048]{1,0:T(8,128)S(1)} %fusion.40, ...), kind=kOutput, calls=%fused_computation.39 | convolution fusion | flops 207618048 | bytes 24215556 | tf_op jit(solution)/shard_map/jrf,jdf->jrd/dot_general | solution.py:146
  191.9 3.9 %all-to-all-start.1 = ((bf16[4,96,2048]{2,1,0:T(8,128)(2,1)}), bf16[4,96,2048]{2,1,0:T(8,128)(2,1)S(1)}, u32[]{:S(2)}, u32[]{:S(2)}) async-start(bf16[4,96,2048]{2,1,0:T(8,128)(2,1)} %bitcast.79), calls=%async_computation.2 | async-start | bytes 3145728 | tf_op jit(solution)/shard_map/all_to_all | solution.py:157
  195.8 0.1 copy.29
  195.9 19.5 %all-to-all-done.1 = bf16[4,96,2048]{2,1,0:T(8,128)(2,1)S(1)} async-done(((bf16[4,96,2048]{2,1,0:T(8,128)(2,1)}), bf16[4,96,2048]{2,1,0:T(8,128)(2,1)S(1)}, u32[]{:S(2)}, u32[]{:S(2)}) %all-to-all-start.1) | async-done | bytes 1572896 | tf_op jit(solution)/shard_map/all_to_all | solution.py:157
  215.5 2.3 %gather_fusion.1 = bf16[256,2048]{1,0:T(8,128)(2,1)} fusion(bf16[384,2048]{1,0:T(8,128)(2,1)S(1)} %bitcast.78, s32[1024]{0:T(1024)S(1)} %pad_clamp_fusion), kind=kCustom, calls=%fused_computation.1 | custom fusion | bytes 2098176 | tf_op jit(solution)/shard_map/gather | solution.py:160
  217.8 2.4 %reshape.227 = f32[128,2,2048]{2,1,0:T(2,128)S(1)} reshape(bf16[256,2048]{1,0:T(8,128)(2,1)} %gather_fusion.1) | data formatting | bytes 3145728 | tf_op jit(solution)/shard_map/convert_element_type | solution.py:160
  220.2 3.9 %multiply_reduce_fusion = bf16[128,2048]{1,0:T(8,128)(2,1)} fusion(f32[128,2,2048]{2,1,0:T(2,128)S(1)} %reshape.227, f32[128,2]{1,0:T(8,128)S(1)} %copy.29), kind=kLoop, calls=%fused_computation.40 | loop fusion | flops 786432 | bytes 2622464 | tf_op jit(solution)/shard_map/reduce_sum | solution.py:162
  (83 shorter events, 0.7 us)
Async XLA Ops:
  7.2 82.8 %copy-start = (bf16[2,128,2048]{2,1,0:T(8,128)(2,1)S(1)}, bf16[2,128,2048]{2,1,0:T(8,128)(2,1)}, u32[]{:S(2)}) copy-start(bf16[2,128,2048]{2,1,0:T(8,128)(2,1)} %param.23) | copy-start | bytes 3145732
  7.2 5.0 %copy-start.2 = (bf16[1,2048,128]{2,1,0:T(8,128)(2,1)S(1)}, bf16[1,2048,128]{2,1,0:T(8,128)(2,1)}, u32[]{:S(2)}) copy-start(bf16[1,2048,128]{2,1,0:T(8,128)(2,1)} %param.31) | copy-start | bytes 1572868
  7.2 9.7 %copy-start.10 = (s32[128,2]{0,1:T(2,128)S(1)}, s32[128,2]{0,1:T(2,128)}, u32[]{:S(2)}) copy-start(s32[128,2]{0,1:T(2,128)} %param.26) | copy-start | bytes 3076
  7.2 11.9 %copy-start.1 = (bf16[128,2048]{1,0:T(8,128)(2,1)S(1)}, bf16[128,2048]{1,0:T(8,128)(2,1)}, u32[]{:S(2)}) copy-start(bf16[128,2048]{1,0:T(8,128)(2,1)} %param.24) | copy-start | bytes 1572868
  7.2 20.9 %copy-start.9 = (f32[2048]{0:T(1024)S(1)}, f32[2048]{0:T(1024)}, u32[]{:S(2)}) copy-start(f32[2048]{0:T(1024)} %param.25) | copy-start | bytes 24580
  7.2 43.1 %all-gather.5.cloned.1.call-start = ((), (), s32[]{:S(2)}) async-start(), calls=%async_computation.3 | async-start | bytes 1310720 | tf_op jit(solution)/shard_map/all_gather | solution.py:69
  9.1 68.9 %all-gather.7.cloned.1.call-start = ((), (), s32[]{:S(2)}) async-start(), calls=%async_computation.4 | async-start | bytes 1310720 | tf_op jit(solution)/shard_map/all_gather | solution.py:70
  10.9 116.5 %all-gather.9.cloned.1.call-start = ((), (), s32[]{:S(2)}) async-start(), calls=%async_computation.6 | async-start | bytes 4718592 | tf_op jit(solution)/shard_map/all_gather | solution.py:136
  11.6 163.3 %all-gather.11.cloned.1.call-start = ((), (), s32[]{:S(2)}) async-start(), calls=%async_computation.7 | async-start | bytes 4718592 | tf_op jit(solution)/shard_map/all_gather | solution.py:137
  12.2 14.5 %collective-permute-start.1 = (bf16[1,2048,128]{2,1,0:T(8,128)(2,1)S(1)}, bf16[1,2048,128]{2,1,0:T(8,128)(2,1)S(1)}, u32[]{:S(2)}, u32[]{:S(2)}) collective-permute-start(bf16[1,2048,128]{2,1,0:T(8,128)(2,1)S(1)} %copy-done.2), channel_id=1, source_target_pairs={{0,1},{1,2},{2,3},{3,4},{4,5},{5,6},{6,7},{7,0},{8,9},{9,10},{10,1... | collective-permute-start | bytes 1572872 | tf_op jit(solution)/shard_map/ppermute | solution.py:18
  12.8 15.5 %collective-permute-start = (bf16[1,2048,128]{2,1,0:T(8,128)(2,1)S(1)}, bf16[1,2048,128]{2,1,0:T(8,128)(2,1)S(1)}, u32[]{:S(2)}, u32[]{:S(2)}) collective-permute-start(bf16[1,2048,128]{2,1,0:T(8,128)(2,1)S(1)} %copy-done.2), channel_id=1, source_target_pairs={{0,7},{1,0},{2,1},{3,2},{4,3},{5,4},{6,5},{7,6},{8,15},{9,8},{10,9... | collective-permute-start | bytes 1572872 | tf_op jit(solution)/shard_map/ppermute | solution.py:20
  26.7 14.2 %copy-start.4 = (bf16[1,2048,128]{2,1,0:T(8,128)(2,1)}, bf16[1,2048,128]{2,1,0:T(8,128)(2,1)S(1)}, u32[]{:S(2)}) copy-start(bf16[1,2048,128]{2,1,0:T(8,128)(2,1)S(1)} %collective-permute-done.1) | copy-start | bytes 1572868
  26.7 11.0 %collective-permute-start.3 = (bf16[1,2048,128]{2,1,0:T(8,128)(2,1)S(1)}, bf16[1,2048,128]{2,1,0:T(8,128)(2,1)}, u32[]{:S(2)}, u32[]{:S(2)}) collective-permute-start(bf16[1,2048,128]{2,1,0:T(8,128)(2,1)S(1)} %collective-permute-done.1), channel_id=1, source_target_pairs={{0,1},{1,2},{2,3},{3,4},{4,5},{5,6},{6,7},{7,0},{8,9},{9,10},{10,1... | collective-permute-start | bytes 1572872 | tf_op jit(solution)/shard_map/ppermute | solution.py:18
  28.3 12.6 %copy-start.6 = (bf16[1,2048,128]{2,1,0:T(8,128)(2,1)}, bf16[1,2048,128]{2,1,0:T(8,128)(2,1)S(1)}, u32[]{:S(2)}) copy-start(bf16[1,2048,128]{2,1,0:T(8,128)(2,1)S(1)} %collective-permute-done) | copy-start | bytes 1572868
  28.3 18.7 %collective-permute-start.2 = (bf16[1,2048,128]{2,1,0:T(8,128)(2,1)S(1)}, bf16[1,2048,128]{2,1,0:T(8,128)(2,1)}, u32[]{:S(2)}, u32[]{:S(2)}) collective-permute-start(bf16[1,2048,128]{2,1,0:T(8,128)(2,1)S(1)} %collective-permute-done), channel_id=1, source_target_pairs={{0,7},{1,0},{2,1},{3,2},{4,3},{5,4},{6,5},{7,6},{8,15},{9,8},{10,9... | collective-permute-start | bytes 1572872 | tf_op jit(solution)/shard_map/ppermute | solution.py:20
  37.7 12.6 %collective-permute-start.5 = (bf16[1,2048,128]{2,1,0:T(8,128)(2,1)}, bf16[1,2048,128]{2,1,0:T(8,128)(2,1)}, u32[]{:S(2)}, u32[]{:S(2)}) collective-permute-start(bf16[1,2048,128]{2,1,0:T(8,128)(2,1)} %collective-permute-done.3), channel_id=1, source_target_pairs={{0,1},{1,2},{2,3},{3,4},{4,5},{5,6},{6,7},{7,0},{8,9},{9,10},{10,1... | collective-permute-start | bytes 1572872 | tf_op jit(solution)/shard_map/ppermute | solution.py:18
  40.9 5.9 %copy-start.8 = (bf16[512,2,128]{2,1,0:T(2,128)(2,1)S(1)}, bf16[512,2,128]{2,1,0:T(2,128)(2,1)}, u32[]{:S(2)}) copy-start(bf16[512,2,128]{2,1,0:T(2,128)(2,1)} %param.18) | copy-start | bytes 786436
  40.9 51.3 %all-to-all-start = ((bf16[4,96,2048]{2,1,0:T(8,128)(2,1)}), bf16[4,96,2048]{2,1,0:T(8,128)(2,1)}, u32[]{:S(2)}, u32[]{:S(2)}) async-start(bf16[4,96,2048]{2,1,0:T(8,128)(2,1)} %bitcast.11), calls=%async_computation.1 | async-start | bytes 3145728 | tf_op jit(solution)/shard_map/all_to_all | solution.py:131
  46.8 177.4 %reduce-scatter.2.cloned.1.call-start = ((), (), s32[]{:S(2)}) async-start(), calls=%async_computation.5 | async-start | bytes 2359296 | tf_op jit(solution)/shard_map/reduce_scatter | solution.py:97
  47.0 139.7 %collective-permute-start.4 = (bf16[1,2048,128]{2,1,0:T(8,128)(2,1)}, bf16[1,2048,128]{2,1,0:T(8,128)(2,1)}, u32[]{:S(2)}, u32[]{:S(2)}) collective-permute-start(bf16[1,2048,128]{2,1,0:T(8,128)(2,1)} %collective-permute-done.2), channel_id=1, source_target_pairs={{0,7},{1,0},{2,1},{3,2},{4,3},{5,4},{6,5},{7,6},{8,15},{9,8},{10,9... | collective-permute-start | bytes 1572872 | tf_op jit(solution)/shard_map/ppermute | solution.py:20
  50.3 138.0 %collective-permute-start.6 = (bf16[1,2048,128]{2,1,0:T(8,128)(2,1)}, bf16[1,2048,128]{2,1,0:T(8,128)(2,1)}, u32[]{:S(2)}, u32[]{:S(2)}) collective-permute-start(bf16[1,2048,128]{2,1,0:T(8,128)(2,1)} %collective-permute-done.5), channel_id=1, source_target_pairs={{0,1},{1,2},{2,3},{3,4},{4,5},{5,6},{6,7},{7,0},{8,9},{9,10},{10,1... | collective-permute-start | bytes 1572872 | tf_op jit(solution)/shard_map/ppermute | solution.py:18
  79.4 10.0 %copy-start.12 = (f32[2]{0:T(128)S(1)}, f32[2]{0:T(128)}, u32[]{:S(2)}) copy-start(f32[2]{0:T(128)} %param.21) | copy-start | bytes 28
  79.4 10.6 %copy-start.13 = (f32[128]{0:T(128)S(1)}, f32[128]{0:T(128)}, u32[]{:S(2)}) copy-start(f32[128]{0:T(128)} %param.22) | copy-start | bytes 1540
  131.9 47.6 %copy-start.3 = (bf16[1,2048,128]{2,1,0:T(8,128)(2,1)S(1)}, bf16[1,2048,128]{2,1,0:T(8,128)(2,1)}, u32[]{:S(2)}) copy-start(bf16[1,2048,128]{2,1,0:T(8,128)(2,1)} %param.31) | copy-start | bytes 1572868
  183.3 1.7 copy-start.5
  185.0 1.0 copy-start.7
  191.9 3.9 %copy-start.11 = (f32[128,2]{0,1:T(2,128)S(1)}, f32[128,2]{0,1:T(2,128)}, u32[]{:S(2)}) copy-start(f32[128,2]{0,1:T(2,128)} %param.28) | copy-start | bytes 3076
  191.9 3.9 %copy-start.14 = (f32[128]{0:T(128)S(1)}, f32[128]{0:T(128)}, u32[]{:S(2)}) copy-start(f32[128]{0:T(128)} %param.27) | copy-start | bytes 1540
  191.9 23.6 %all-to-all-start.1 = ((bf16[4,96,2048]{2,1,0:T(8,128)(2,1)}), bf16[4,96,2048]{2,1,0:T(8,128)(2,1)S(1)}, u32[]{:S(2)}, u32[]{:S(2)}) async-start(bf16[4,96,2048]{2,1,0:T(8,128)(2,1)} %bitcast.79), calls=%async_computation.2 | async-start | bytes 3145728 | tf_op jit(solution)/shard_map/all_to_all | solution.py:157
Sparse Core Ops, SparseCore 0:
  10.5 29.2 all-gather.4
  41.6 36.3 all-gather.6
  79.6 47.8 all-gather.8
  128.9 46.0 all-gather.10
  177.6 34.1 reduce-scatter.1
